TPU v7x, 256 devices: a whole 4x4x8 slice. The times are simulated.
256 devices in a mesh: sp: 64 (over z, y, core), tp: 4 (over x).
Axes of the slice: x: 4, y: 4, z: 8, core: 2. Of those that a mesh axis runs over, the one named last changes fastest.
Arguments:
- queries: bfloat16 [32768, 1024], P('sp', 'tp'), may hold values from -6 to 6
- keys: bfloat16 [32768, 1024], P('sp', 'tp'), may hold values from -6 to 6
- values: bfloat16 [32768, 1024], P('sp', 'tp'), may hold values from -6 to 6
- output_gate_logits: bfloat16 [32768, 1024], P('sp', 'tp'), may hold values from -6 to 6
- input_gate_log: float32 [32768, 8], P('sp', 'tp'), may hold values from -5 to 125
- forget_gate_logits: float32 [32768, 8], P('sp', 'tp')
- extra_decay_log: float32 [32768, 8], P('sp', 'tp'), may hold values from -1 to 0
- document: int32 [32768], P('sp'), may hold values from 0 to 31, never falling along the last dimension, each value on 1 to 2048 neighbouring positions
- residual: bfloat16 [32768, 2048], P('sp', 'tp'), may hold values from -16 to 16
- cell_norm_gain: bfloat16 [1024], P('tp'), may hold values from 0.099609375 to 1.8984375
- output_weight: bfloat16 [1024, 2048], P('tp'), may hold values from -0.1875 to 0.1875
- mixer_norm_gain: bfloat16 [2048], P('tp'), may hold values from 0.099609375 to 1.8984375
- up_weight: bfloat16 [2048, 8192], P('sp', 'tp'), may hold values from -0.125 to 0.125
- down_weight: bfloat16 [8192, 2048], P('tp', 'sp'), may hold values from -0.0625 to 0.0625
Outputs:
- layer_out: bfloat16 [32768, 2048], P('sp', 'tp')
All inputs are finite; a program needn't handle non-finite values.
Results may differ from a plain program's by a relative error of at most 0.015.
Values may be sent and summed in bfloat16 or wider, within the bound.
No kernel may reach another device: no remote copies, remote signals or barrier semaphores. Data moves between devices by JAX's collectives and lax.ppermute only.
A program may use at most 128 MiB of HBM per device.

v0:
```python
import jax
import jax.numpy as jnp
from jax import lax
from jax.sharding import Mesh
from jax.sharding import PartitionSpec as P

DH = 128
BLOCK = 128
SP = ("sp_0", "sp_1", "sp_2")
NEG = -1e30
EPS = 1e-06


def sent_to_all(value, axis):
    copies = jnp.broadcast_to(value, (lax.axis_size(axis), *value.shape))
    return lax.all_to_all(copies, axis, split_axis=0, concat_axis=0, tiled=True)


def of_everyone(value, axis):
    return sent_to_all(value, axis).sum(axis=0)


def rows_first(arrays, axis, dims):
    turned = [jnp.moveaxis(a, dim, 0) for a, dim in zip(arrays, dims)]
    widths = [t[0].size for t in turned]
    both = jnp.concatenate([t.reshape(-1, w) for t, w in zip(turned, widths)], axis=1)
    whole = lax.all_gather(both, axis, axis=0, tiled=True)
    parts = jnp.split(whole, [sum(widths[:k]) for k in range(1, len(widths))], axis=1)
    return tuple(
        (
            jnp.moveaxis(b.reshape(-1, *t.shape[1:]), 0, dim)
            for b, t, dim in zip(parts, turned, dims)
        )
    )


def nothing_yet(value, identity):
    return jax.tree.map(
        lambda a, e: jnp.broadcast_to(jnp.asarray(e, a.dtype), a.shape), value, identity
    )


def all_in_one(value, axis):
    leaves = jax.tree.leaves(value)
    order = sorted(range(len(leaves)), key=lambda k: -leaves[k].size)
    width = (1, *leaves[order[0]].shape)[-1]
    lines = [
        jnp.pad(leaves[k].reshape(-1), (0, -leaves[k].size % width)).reshape(-1, width)
        for k in order
    ]
    both, at, found = (lax.all_gather(jnp.concatenate(lines), axis), 0, {})
    for k, line in zip(order, lines):
        piece = both[:, at : at + len(line)].reshape(len(both), -1)
        found[k] = piece[:, : leaves[k].size].reshape(-1, *leaves[k].shape)
        at += len(line)
    numbers = iter(range(len(leaves)))
    return jax.tree.map(lambda _: found[next(numbers)], value)


def collected_alike(value, axis):
    leaves, found = (jax.tree.leaves(value), {})
    for leading, a in enumerate(leaves):
        if leading not in found:
            alike = [k for k, b in enumerate(leaves) if b.dtype == a.dtype]
            got = (
                all_in_one([leaves[k] for k in alike], axis)
                if len(alike) > 1
                else [lax.all_gather(a, axis)]
            )
            for k, b in zip(alike, got):
                found[k] = b
    numbers = iter(range(len(leaves)))
    return jax.tree.map(lambda _: found[next(numbers)], value)


def entering(value, axes, combine, identity):
    before = start = nothing_yet(value, identity)
    subtotal = value
    for axis in reversed(axes):
        count, index = (lax.axis_size(axis), lax.axis_index(axis))
        pieces = collected_alike(subtotal, axis)
        inside, subtotal = (start, start)
        for k in range(count):
            passed = k < index
            subtotal = combine(subtotal, jax.tree.map(lambda part: part[k], pieces))
            inside = jax.tree.map(lambda new, old: jnp.where(passed, new, old), subtotal, inside)
        before = combine(inside, before)
    return before


def cut_along(value, dim, count):
    lengths = value.shape
    parts = value.reshape(*lengths[:dim], count, lengths[dim] // count, *lengths[dim + 1 :])
    return jnp.moveaxis(parts, dim, 0)


def summed_on_arrival(value, axis, dim):
    parts = cut_along(value, dim, lax.axis_size(axis))
    arrived = lax.all_to_all(parts, axis, split_axis=0, concat_axis=0, tiled=True)
    return arrived.astype(jnp.float32).sum(axis=0)


def joined_along(parts, dim):
    parts = jnp.moveaxis(parts, 0, dim)
    lengths = parts.shape
    return parts.reshape(*lengths[:dim], lengths[dim] * lengths[dim + 1], *lengths[dim + 2 :])


def gathered_copies(value, axis, dim):
    return joined_along(sent_to_all(value, axis), dim)


def block_terms(carry, inputs):
    memory, normer, stabil, last_doc = carry
    q_blk, k_blk, v_blk, gate_in, gate_log, doc_blk = inputs
    length = doc_blk.shape[0]
    causal = jnp.arange(length)[:, None] >= jnp.arange(length)[None, :]
    cumulative = jnp.cumsum(gate_log, axis=-1)
    same_doc = (doc_blk[:, None] == doc_blk[None, :]) & causal
    pair_log = cumulative[:, :, None] - cumulative[:, None, :] + gate_in[:, None, :]
    pair_log = jnp.where(same_doc[None], pair_log, NEG)
    live_rows = doc_blk == last_doc
    carried_log = jnp.where(live_rows[None, :], cumulative + stabil[:, None], NEG)
    peak_log = jnp.maximum(carried_log, jnp.max(pair_log, axis=-1))
    weights = jnp.exp(pair_log - peak_log[:, :, None])
    carried = jnp.exp(carried_log - peak_log)
    scores = jnp.einsum("htd,hsd->hts", q_blk, k_blk) * weights
    numerator = carried[:, :, None] * jnp.einsum("htd,hde->hte", q_blk, memory)
    numerator = numerator + jnp.einsum("hts,hse->hte", scores, v_blk)
    denominator = carried * jnp.einsum("htd,hd->ht", q_blk, normer) + jnp.sum(scores, axis=-1)
    end_doc = doc_blk[-1]
    end_cum = cumulative[:, -1]
    keep_log = jnp.where(
        (doc_blk == end_doc)[None, :], end_cum[:, None] - cumulative + gate_in, NEG
    )
    old_log = jnp.where(last_doc == end_doc, end_cum + stabil, NEG)
    new_stab = jnp.maximum(old_log, jnp.max(keep_log, axis=-1))
    scaled = jnp.exp(keep_log - new_stab[:, None])
    decayed = jnp.exp(old_log - new_stab)
    memory = decayed[:, None, None] * memory + jnp.einsum("hs,hsd,hse->hde", scaled, k_blk, v_blk)
    normer = decayed[:, None] * normer + jnp.einsum("hs,hsd->hd", scaled, k_blk)
    return ((memory, normer, new_stab, end_doc), (numerator, denominator, peak_log, cumulative))


def split_heads(source, blocks):
    return source.astype(jnp.float32).reshape(blocks, BLOCK, -1, DH).transpose(0, 2, 1, 3)


def split_gates(source, blocks):
    return source.reshape(blocks, BLOCK, -1).transpose(0, 2, 1)


def within_block_pass(
    queries, keys, values, input_gate_log, forget_gate_logits, extra_decay_log, document
):
    blocks = queries.shape[0] // BLOCK
    head_count = queries.shape[1] // DH
    query_heads = split_heads(queries, blocks) * DH ** (-0.5)
    forget_log_values = jax.nn.log_sigmoid(forget_gate_logits) + extra_decay_log
    inputs = (
        query_heads,
        split_heads(keys, blocks),
        split_heads(values, blocks),
        split_gates(input_gate_log, blocks),
        split_gates(forget_log_values, blocks),
        document.reshape(blocks, BLOCK),
    )
    initial = (
        jnp.zeros((head_count, DH, DH), jnp.float32),
        jnp.zeros((head_count, DH), jnp.float32),
        jnp.full((head_count,), NEG, jnp.float32),
        jnp.array(-1, jnp.int32),
    )
    final_state, output_rows = lax.scan(block_terms, initial, inputs)
    return (query_heads, final_state, output_rows)


def head_mix(cell_out, output_gate_logits, cell_norm_gain):
    row_count = output_gate_logits.shape[0]
    head_count = cell_out.shape[1]
    hidden = cell_out.transpose(0, 2, 1, 3).reshape(row_count, head_count * DH)
    squares = of_everyone(jnp.sum(hidden * hidden, axis=1), "tp")
    inverse = lax.rsqrt(squares / (head_count * DH * lax.axis_size("tp")) + EPS)
    gated = jax.nn.sigmoid(output_gate_logits.astype(jnp.float32))
    gains = cell_norm_gain.astype(jnp.float32)
    return (gated * hidden * inverse[:, None] * gains[None, :]).astype(jnp.bfloat16)


def join_states(earlier, later):
    mem_a, norm_a, stab_a, log_a, first_a, last_a = earlier
    mem_b, norm_b, stab_b, log_b, first_b, last_b = later
    joined = last_a == last_b
    stab_ab = jnp.where(joined, jnp.maximum(log_b + stab_a, stab_b), stab_b)
    weight_a = jnp.where(joined, jnp.exp(log_b + stab_a - stab_ab), 0.0)
    weight_b = jnp.exp(stab_b - stab_ab)
    memory = weight_a[:, None, None] * mem_a + weight_b[:, None, None] * mem_b
    normer = weight_a[:, None] * norm_a + weight_b[:, None] * norm_b
    blank_b = last_b < 0
    memory = jnp.where(blank_b, mem_a, memory)
    normer = jnp.where(blank_b, norm_a, normer)
    stabil = jnp.where(blank_b, stab_a, stab_ab)
    first_doc = jnp.where(first_a < 0, first_b, first_a)
    last_doc = jnp.where(blank_b, last_a, last_b)
    return (memory, normer, stabil, log_a + log_b, first_doc, last_doc)


def local(
    queries,
    keys,
    values,
    output_gate_logits,
    input_gate_log,
    forget_gate_logits,
    extra_decay_log,
    document,
    residual,
    cell_norm_gain,
    output_weight,
    mixer_norm_gain,
    up_weight,
    down_weight,
):
    up_whole, down_whole = rows_first((up_weight, down_weight), SP, (0, 1))
    query_heads, final_state, output_rows = within_block_pass(
        queries, keys, values, input_gate_log, forget_gate_logits, extra_decay_log, document
    )
    numerator, denominator, peak_log, cumulative = output_rows
    memory, normer, stabil, last_doc = final_state
    step_logs = cumulative[:, :, -1]
    offsets = jnp.cumsum(step_logs, axis=0) - step_logs
    through = cumulative + offsets[:, :, None]
    summary = (memory, normer, stabil, jnp.sum(step_logs, axis=0), document[0], last_doc)
    identity = (
        jnp.zeros_like(memory),
        jnp.zeros_like(normer),
        jnp.full_like(stabil, NEG),
        jnp.zeros_like(stabil),
        jnp.array(-1, jnp.int32),
        jnp.array(-1, jnp.int32),
    )
    prefix = entering(summary, SP, join_states, identity)
    doc_blocks = document.reshape(-1, BLOCK)
    carried_log = jnp.where(
        (doc_blocks == prefix[5])[:, None, :], through + prefix[2][None, :, None], NEG
    )
    merged_peak = jnp.maximum(peak_log, carried_log)
    own_weight = jnp.exp(peak_log - merged_peak)
    far_weight = jnp.exp(carried_log - merged_peak)
    numerator = own_weight[..., None] * numerator + far_weight[..., None] * jnp.einsum(
        "nhtd,hde->nhte", query_heads, prefix[0]
    )
    denominator = own_weight * denominator + far_weight * jnp.einsum(
        "nhtd,hd->nht", query_heads, prefix[1]
    )
    cell_out = numerator / jnp.maximum(jnp.abs(denominator), 1.0)[..., None]
    mixed = head_mix(cell_out, output_gate_logits, cell_norm_gain)
    head_terms = jnp.dot(mixed, output_weight, preferred_element_type=jnp.float32)
    width = residual.shape[1]
    model_width = width * lax.axis_size("tp")
    own_sum = summed_on_arrival(head_terms.astype(jnp.bfloat16), "tp", 1)
    first_sum = (residual.astype(jnp.float32) + own_sum).astype(jnp.bfloat16)
    first_wide = lax.optimization_barrier(first_sum).astype(jnp.float32)
    squares = of_everyone(jnp.sum(first_wide * first_wide, axis=1), "tp")
    inverse = lax.rsqrt(squares / model_width + EPS)
    normed_own = (first_wide * inverse[:, None] * mixer_norm_gain.astype(jnp.float32)).astype(
        jnp.bfloat16
    )
    normed_full = gathered_copies(normed_own, "tp", 1)
    hidden = jnp.dot(normed_full, up_whole, preferred_element_type=jnp.float32)
    squared = jnp.square(jax.nn.relu(hidden)).astype(jnp.bfloat16)
    channel = jnp.dot(squared, down_whole, preferred_element_type=jnp.float32)
    own_channel = summed_on_arrival(channel.astype(jnp.bfloat16), "tp", 1)
    return (lax.optimization_barrier(first_sum).astype(jnp.float32) + own_channel).astype(
        jnp.bfloat16
    )


def solution(mesh):
    split = Mesh(mesh.devices.reshape(8, 4, 2, mesh.shape["tp"]), ("sp_0", "sp_1", "sp_2", "tp"))
    return jax.shard_map(
        local,
        mesh=split,
        in_specs=(
            P(SP, "tp"),
            P(SP, "tp"),
            P(SP, "tp"),
            P(SP, "tp"),
            P(SP, "tp"),
            P(SP, "tp"),
            P(SP, "tp"),
            P(SP),
            P(SP, "tp"),
            P("tp"),
            P("tp", None),
            P("tp"),
            P(SP, "tp"),
            P("tp", SP),
        ),
        out_specs=P(SP, "tp"),
        check_vma=False,
    )
```

profile of v0, /device:TPU:1, one launch (start us, length us, event | category | flops | bytes accessed | tf_op | source)
XLA Modules:
  0.0 278.6 jit_solution(83311342895520995)
XLA Ops:
  6.7 1.1 convert_multiply_fusion.2
  7.8 1.2 reshape.3525
  9.0 1.0 reshape.3526
  10.6 25.0 %while.25 = (s32[]{:T(128)}, f32[2,128,128]{2,1,0:T(8,128)S(1)}, f32[2,128]{1,0:T(2,128)S(1)}, f32[2]{0:T(128)S(1)}, s32[]{:T(128)}, /*index=5*/f32[4,2,128,128]...) while((s32[]{:T(128)}, f32[2,128,128]{2,1,0:T(8,128)S(1)}, ...), condition=%wide.region_5.6_spmd.clone, body=%wide.region_0.5_spmd.clone.sunk | while | flops 34361868 | bytes 2780512 | solution.py:174
  37.7 4.7 %all-reduce.6 = s32[4]{0:T(128)S(1)} all-reduce(s32[4]{0:T(128)S(1)} %fusion.253), channel_id=2, replica_groups=mesh['sp_0'=8,'sp_1'=4,'sp_2'=2,'tp'=4] {'sp_2'}, use_global_device_ids=true, to_apply=%add.6 | all-reduce | flops 4 | bytes 32
  49.9 5.4 %all-reduce.7 = s32[8]{0:T(128)S(1)} all-reduce(s32[8]{0:T(128)S(1)} %fusion.254), channel_id=3, replica_groups=mesh['sp_0'=8,'sp_1'=4,'sp_2'=2,'tp'=4] {'sp_1'}, use_global_device_ids=true, to_apply=%add.7 | all-reduce | flops 8 | bytes 64
  57.4 4.0 %all-gather.6 = f32[2,260,128]{2,1,0:T(8,128)S(1)} all-gather(f32[1,260,128]{2,1,0:T(8,128)S(1)} %maximum_bitcast_fusion), channel_id=5, replica_groups=mesh['sp_0'=8,'sp_1'=4,'sp_2'=2,'tp'=4] {'sp_2'}, dimensions={0}, use_global_device_ids=true | all-gather | bytes 399360 | tf_op jit(solution)/shard_map/all_gather | solution.py:51
  61.8 9.9 %all-gather.7 = f32[4,260,128]{2,1,0:T(8,128)S(1)} all-gather(f32[1,260,128]{2,1,0:T(8,128)S(1)} %maximum_bitcast_fusion.1), channel_id=6, replica_groups=mesh['sp_0'=8,'sp_1'=4,'sp_2'=2,'tp'=4] {'sp_1'}, dimensions={0}, use_global_device_ids=true | all-gather | bytes 665600 | tf_op jit(solution)/shard_map/all_gather | solution.py:51
  84.4 13.2 %all-reduce.8 = s32[16]{0:T(128)S(1)} all-reduce(s32[16]{0:T(128)S(1)} %fusion.255), channel_id=4, replica_groups=mesh['sp_0'=8,'sp_1'=4,'sp_2'=2,'tp'=4] {'sp_0'}, use_global_device_ids=true, to_apply=%add.8 | all-reduce | flops 16 | bytes 128
  117.3 1.4 fusion.280
  122.5 0.9 add_select_fusion.4
  123.7 2.1 multiply_reduce_fusion
  126.4 3.9 %all-to-all-start = ((f32[4,1,512]{2,1,0:T(1,128)}), f32[4,1,512]{2,1,0:T(1,128)S(1)}, u32[]{:S(2)}, u32[]{:S(2)}) async-start(f32[4,1,512]{2,1,0:T(1,128)} %broadcast_in_dim.110), calls=%async_computation | async-start | bytes 16384 | tf_op jit(solution)/shard_map/all_to_all | solution.py:16
  130.5 3.9 %all-to-all-done = f32[4,1,512]{2,1,0:T(1,128)S(1)} async-done(((f32[4,1,512]{2,1,0:T(1,128)}), f32[4,1,512]{2,1,0:T(1,128)S(1)}, u32[]{:S(2)}, u32[]{:S(2)}) %all-to-all-start) | async-done | bytes 8224 | tf_op jit(solution)/shard_map/all_to_all | solution.py:16
  134.5 1.7 convolution_convert_fusion
  136.4 20.6 %all_to_all.27 = bf16[4,512,512]{2,1,0:T(8,128)(2,1)S(1)} all-to-all(bf16[4,512,512]{2,1,0:T(8,128)(2,1)S(1)} %bitcast.687), channel_id=1, replica_groups=mesh['sp_0'=8,'sp_1'=4,'sp_2'=2,'tp'=4] {'tp'}, dimensions={0} | all-to-all | bytes 4194304 | tf_op jit(solution)/shard_map/all_to_all | solution.py:99
  159.0 3.2 %all-to-all-start.2 = ((f32[4,1,512]{2,1,0:T(1,128)}), f32[4,1,512]{2,1,0:T(1,128)S(1)}, u32[]{:S(2)}, u32[]{:S(2)}) async-start(f32[4,1,512]{2,1,0:T(1,128)} %broadcast_in_dim.111), calls=%async_computation.2 | async-start | bytes 16384 | tf_op jit(solution)/shard_map/all_to_all | solution.py:16
  162.3 4.1 %all-to-all-done.2 = f32[4,1,512]{2,1,0:T(1,128)S(1)} async-done(((f32[4,1,512]{2,1,0:T(1,128)}), f32[4,1,512]{2,1,0:T(1,128)S(1)}, u32[]{:S(2)}, u32[]{:S(2)}) %all-to-all-start.2) | async-done | bytes 8224 | tf_op jit(solution)/shard_map/all_to_all | solution.py:16
  167.1 19.4 %all_to_all.28 = bf16[4,512,512]{1,2,0:T(8,128)(2,1)} all-to-all(bf16[4,512,512]{1,2,0:T(8,128)(2,1)S(1)} %broadcast_in_dim.112), channel_id=1, replica_groups=mesh['sp_0'=8,'sp_1'=4,'sp_2'=2,'tp'=4] {'tp'}, dimensions={0} | all-to-all | bytes 4194304 | tf_op jit(solution)/shard_map/all_to_all | solution.py:16
  186.5 35.9 %all-gather.12.cloned.1.call-done = bf16[2048,4096]{1,0:T(8,128)(2,1)} async-done(((bf16[32,4096]{1,0:T(8,128)(2,1)}), bf16[2048,4096]{1,0:T(8,128)(2,1)}) %all-gather.12.cloned.1.call-update) | async-done | bytes 16777232 | tf_op jit(solution)/shard_map/all_gather | solution.py:27
  222.4 16.6 %fusion.24 = bf16[512,2048]{1,0:T(8,128)(2,1)} fusion(bf16[2048,4096]{1,0:T(8,128)(2,1)} %all-gather.12.cloned.1.call-done, bf16[512,2048]{0,1:T(8,128)(2,1)} %bitcast.691), kind=kOutput, calls=%fused_computation.56 | convolution fusion | flops 8594128896 | bytes 20971520 | tf_op jit(solution)/shard_map/dot_general | solution.py:271
  239.0 1.8 copy.230
  240.8 29.7 %all_to_all.29 = bf16[4,512,512]{2,1,0:T(8,128)(2,1)S(1)} all-to-all(bf16[4,512,512]{2,1,0:T(8,128)(2,1)S(1)} %bitcast.688), channel_id=1, replica_groups=mesh['sp_0'=8,'sp_1'=4,'sp_2'=2,'tp'=4] {'tp'}, dimensions={0} | all-to-all | bytes 4194304 | tf_op jit(solution)/shard_map/all_to_all | solution.py:99
  270.8 1.0 fusion.37
  (230 shorter events, 40.3 us)
Async XLA Ops:
  6.5 127.9 %copy-start = (bf16[256,2048]{1,0:T(8,128)(2,1)S(1)}, bf16[256,2048]{1,0:T(8,128)(2,1)}, u32[]{:S(2)}) copy-start(bf16[256,2048]{1,0:T(8,128)(2,1)} %param.26) | copy-start | bytes 3145732
  6.5 3.5 %copy-start.6 = (s32[512]{0:T(512)S(1)}, s32[512]{0:T(512)}, u32[]{:S(2)}) copy-start(s32[512]{0:T(512)} %param.23) | copy-start | bytes 6148
  6.5 4.0 %copy-start.8 = (f32[512,2]{0,1:T(2,128)S(1)}, f32[512,2]{0,1:T(2,128)}, u32[]{:S(2)}) copy-start(f32[512,2]{0,1:T(2,128)} %param.21) | copy-start | bytes 12292
  6.5 4.0 %copy-start.7 = (f32[512,2]{0,1:T(2,128)S(1)}, f32[512,2]{0,1:T(2,128)}, u32[]{:S(2)}) copy-start(f32[512,2]{0,1:T(2,128)} %param.22) | copy-start | bytes 12292
  6.5 110.7 %all-gather.14.cloned.1.call-start = ((), (), s32[]{:S(2)}) async-start(), calls=%async_computation.6 | async-start | bytes 1216512 | tf_op jit(solution)/shard_map/all_gather | solution.py:51
  10.6 25.1 %copy-start.13 = (u32[256]{0:T(256)S(1)}, u32[256]{0:T(256)}, u32[]{:S(2)}) copy-start(u32[256]{0:T(256)} %constant.114) | copy-start | bytes 3076
  10.6 35.4 %copy-start.12 = (u32[256]{0:T(256)S(1)}, u32[256]{0:T(256)}, u32[]{:S(2)}) copy-start(u32[256]{0:T(256)} %constant.119) | copy-start | bytes 3076
  35.6 42.9 %copy-start.4 = (bf16[2048,32]{0,1:T(8,128)(2,1)S(1)}, bf16[2048,32]{0,1:T(8,128)(2,1)}, u32[]{:S(2)}) copy-start(bf16[2048,32]{0,1:T(8,128)(2,1)} %param.29) | copy-start | bytes 393220
  35.6 42.9 %copy-start.5 = (bf16[32,2048]{1,0:T(8,128)(2,1)S(1)}, bf16[32,2048]{1,0:T(8,128)(2,1)}, u32[]{:S(2)}) copy-start(bf16[32,2048]{1,0:T(8,128)(2,1)} %param.28) | copy-start | bytes 393220
  49.2 33.3 %copy-start.11 = (u32[256]{0:T(256)S(1)}, u32[256]{0:T(256)}, u32[]{:S(2)}) copy-start(u32[256]{0:T(256)} %constant.124) | copy-start | bytes 3076
  78.5 143.9 %all-gather.12.cloned.1.call-start = ((), (), s32[]{:S(2)}) async-start(), calls=%async_computation.5 | async-start | bytes 17039360 | tf_op jit(solution)/shard_map/all_gather | solution.py:27
  119.4 4.3 %copy-start.2 = (f32[2,128,128]{1,2,0:T(8,128)S(1)}, f32[2,128,128]{1,2,0:T(8,128)}, u32[]{:S(2)}) copy-start(f32[2,128,128]{1,2,0:T(8,128)} %copy.162) | copy-start | bytes 393220
  120.1 3.6 %copy-start.3 = (f32[2,128,128]{1,2,0:T(8,128)S(1)}, f32[2,128,128]{1,2,0:T(8,128)}, u32[]{:S(2)}) copy-start(f32[2,128,128]{1,2,0:T(8,128)} %copy.163) | copy-start | bytes 393220
  123.7 6.6 %copy-start.10 = (bf16[256]{0:T(256)(128)(2,1)S(1)}, bf16[256]{0:T(256)(128)(2,1)}, u32[]{:S(2)}) copy-start(bf16[256]{0:T(256)(128)(2,1)} %param.25) | copy-start | bytes 1540
  126.4 8.0 %all-to-all-start = ((f32[4,1,512]{2,1,0:T(1,128)}), f32[4,1,512]{2,1,0:T(1,128)S(1)}, u32[]{:S(2)}, u32[]{:S(2)}) async-start(f32[4,1,512]{2,1,0:T(1,128)} %broadcast_in_dim.110), calls=%async_computation | async-start | bytes 16384 | tf_op jit(solution)/shard_map/all_to_all | solution.py:16
  157.1 1.0 copy-start.1
  158.1 4.2 %copy-start.9 = (bf16[512]{0:T(512)(128)(2,1)S(1)}, bf16[512]{0:T(512)(128)(2,1)}, u32[]{:S(2)}) copy-start(bf16[512]{0:T(512)(128)(2,1)} %param.27) | copy-start | bytes 3076
  159.0 7.4 %all-to-all-start.2 = ((f32[4,1,512]{2,1,0:T(1,128)}), f32[4,1,512]{2,1,0:T(1,128)S(1)}, u32[]{:S(2)}, u32[]{:S(2)}) async-start(f32[4,1,512]{2,1,0:T(1,128)} %broadcast_in_dim.111), calls=%async_computation.2 | async-start | bytes 16384 | tf_op jit(solution)/shard_map/all_to_all | solution.py:16
Sparse Core Ops, SparseCore 0:
  78.6 38.6 all-gather.13
  120.0 102.3 all-gather.11
where the time goes:
time: 280 us; the launch traced here: 279 us
  blocking collectives  107 us (38%)
  between operations  46.7 us (17%)
  waiting for transfers between devices  44.1 us (16%)
  local copies, waits for them, and re-layouts  26.7 us (10%)
  matrix products  25.1 us (9%)
  other arithmetic  17 us (6%)
  starting transfers between devices  7.18 us (3%)
  loops' own time  4.89 us (2%)
    all_to_all x2, blocking collectives, summed_on_arrival(): lax.all_to_all(parts, axis, split_axis=0, concat_axis=0, tiled=True)  50.3 us
    all_gather x1, waiting for transfers between devices, rows_first(): whole = lax.all_gather(both, axis, axis=0, tiled=True)  35.9 us
    unnamed x3, blocking collectives  23.2 us
    all_to_all x1, blocking collectives, sent_to_all(): return lax.all_to_all(copies, axis, split_axis=0, concat_axis=0, tiled=True)  19.4 us
    dot_general x1, matrix products, local(): channel = jnp.dot(squared, down_whole, preferred_element_type=jnp.float32)  16.6 us
    all_gather x2, blocking collectives, all_in_one(): both, at, found = (lax.all_gather(jnp.concatenate(lines), axis), 0, {})  13.9 us
    all_to_all x2, waiting for transfers between devices, sent_to_all(): return lax.all_to_all(copies, axis, split_axis=0, concat_axis=0, tiled=True)  8.02 us
    all_to_all x2, starting transfers between devices, sent_to_all(): return lax.all_to_all(copies, axis, split_axis=0, concat_axis=0, tiled=True)  7.1 us
  transfers between devices with their start and end apart: 4, of which 4 were waited for; matrix products, arithmetic and copies ran while one was open for 7% of the time, Pallas kernels for 0%

commit v1 on v0

--- a/solution.py
+++ b/solution.py
@@ -24,7 +24,9 @@
     turned = [jnp.moveaxis(a, dim, 0) for a, dim in zip(arrays, dims)]
     widths = [t[0].size for t in turned]
     both = jnp.concatenate([t.reshape(-1, w) for t, w in zip(turned, widths)], axis=1)
-    whole = lax.all_gather(both, axis, axis=0, tiled=True)
+    whole = jnp.concatenate(
+        lax.all_to_all(jnp.stack([both] * lax.axis_size(axis)), axis, 0, 0), axis=0
+    )
     parts = jnp.split(whole, [sum(widths[:k]) for k in range(1, len(widths))], axis=1)
     return tuple(
         (

time: 280 us -> 634 us (2.26)
  blocking collectives: 107 us -> 469 us
  waiting for transfers between devices: 44.1 us -> 27.2 us
    all_to_all x1, blocking collectives: 19.4 us -> 383 us  [rows_first(): lax.all_to_all(jnp.stack([both] * lax.axis_size(axis)), axis, 0, 0)]
    all_gather x1 -> x0, waiting for transfers between devices: 35.9 us -> none  [rows_first(): whole = lax.all_gather(both, axis, axis=0, tiled=True)]
    all_to_all x2 -> x3, waiting for transfers between devices: 8.02 us -> 24.9 us  [sent_to_all(): return lax.all_to_all(copies, axis, split_axis=0, concat_axis=0, tiled=True)]
  transfers between devices with their start and end apart: 4 -> 4, of which waited for: 4 -> 4; matrix products, arithmetic and copies ran while one was open for 7% -> 0% of each run, Pallas kernels for 0% -> 0%
where the time goes in v1:
time: 634 us; the launch traced here: 631 us
  blocking collectives  469 us (74%)
  between operations  47.9 us (8%)
  local copies, waits for them, and re-layouts  27.8 us (4%)
  waiting for transfers between devices  27.2 us (4%)
  matrix products  25 us (4%)
  other arithmetic  16.6 us (3%)
  starting transfers between devices  11.8 us (2%)
    all_to_all x1, blocking collectives, rows_first(): lax.all_to_all(jnp.stack([both] * lax.axis_size(axis)), axis, 0, 0)  383 us
    all_to_all x2, blocking collectives, summed_on_arrival(): lax.all_to_all(parts, axis, split_axis=0, concat_axis=0, tiled=True)  48.3 us
    all_to_all x3, waiting for transfers between devices, sent_to_all(): return lax.all_to_all(copies, axis, split_axis=0, concat_axis=0, tiled=True)  24.9 us
    unnamed x3, blocking collectives  23.2 us
    dot_general x1, matrix products, local(): channel = jnp.dot(squared, down_whole, preferred_element_type=jnp.float32)  16.6 us
    all_gather x2, blocking collectives, all_in_one(): both, at, found = (lax.all_gather(jnp.concatenate(lines), axis), 0, {})  13.9 us
  transfers between devices with their start and end apart: 4, of which 4 were waited for; matrix products, arithmetic and copies ran while one was open for 0% of the time, Pallas kernels for 0%

profile of v1, /device:TPU:1, one launch (start us, length us, event | category | flops | bytes accessed | tf_op | source)
XLA Modules:
  0.0 630.7 jit_solution(814193050342886054)
XLA Ops:
  6.7 1.3 reshape.3531
  10.7 26.0 %while.25 = (s32[]{:T(128)}, f32[2,128,128]{2,1,0:T(8,128)S(1)}, f32[2,128]{1,0:T(2,128)S(1)}, f32[2]{0:T(128)S(1)}, s32[]{:T(128)}, /*index=5*/f32[4,2,128,128]...) while((s32[]{:T(128)}, f32[2,128,128]{2,1,0:T(8,128)S(1)}, ...), condition=%wide.region_5.6_spmd.clone, body=%wide.region_0.5_spmd.clone.sunk | while | flops 34361868 | bytes 2780012 | solution.py:176
  38.8 4.7 all-reduce.6
  51.4 5.4 all-reduce.7
  59.0 4.0 all-gather.6
  63.4 9.9 %all-gather.7 = f32[4,260,128]{2,1,0:T(8,128)S(1)} all-gather(f32[1,260,128]{2,1,0:T(8,128)S(1)} %maximum_bitcast_fusion.1), channel_id=6, replica_groups=mesh['sp_0'=8,'sp_1'=4,'sp_2'=2,'tp'=4] {'sp_1'}, dimensions={0}, use_global_device_ids=true | all-gather | bytes 665600 | tf_op jit(solution)/shard_map/all_gather | solution.py:53
  85.7 13.2 %all-reduce.8 = s32[16]{0:T(128)S(1)} all-reduce(s32[16]{0:T(128)S(1)} %fusion.255), channel_id=4, replica_groups=mesh['sp_0'=8,'sp_1'=4,'sp_2'=2,'tp'=4] {'sp_0'}, use_global_device_ids=true, to_apply=%add.8 | all-reduce | flops 16 | bytes 128
  116.1 2.3 all-gather.11.cloned.1.call-done
  120.7 1.4 fusion.280
  124.9 2.0 multiply_reduce_fusion
  127.5 3.9 all-to-all-start
  131.7 3.9 all-to-all-done
  135.6 1.7 convolution_convert_fusion
  137.6 21.7 %all_to_all.32 = bf16[4,512,512]{2,1,0:T(8,128)(2,1)S(1)} all-to-all(bf16[4,512,512]{2,1,0:T(8,128)(2,1)S(1)} %bitcast.689), channel_id=1, replica_groups=mesh['sp_0'=8,'sp_1'=4,'sp_2'=2,'tp'=4] {'tp'}, dimensions={0} | all-to-all | bytes 4194304 | tf_op jit(solution)/shard_map/all_to_all | solution.py:101
  161.2 3.2 all-to-all-start.2
  164.5 4.1 all-to-all-done.2
  169.0 1.5 broadcast_in_dim.112
  170.6 4.6 all-to-all-start.3
  175.2 16.9 %all-to-all-done.3 = bf16[4,512,512]{1,2,0:T(8,128)(2,1)} async-done(((bf16[4,512,512]{1,2,0:T(8,128)(2,1)}), bf16[4,512,512]{1,2,0:T(8,128)(2,1)}, u32[]{:S(2)}, u32[]{:S(2)}) %all-to-all-start.3) | async-done | bytes 2097184 | tf_op jit(solution)/shard_map/all_to_all | solution.py:16
  192.1 2.1 stack.2
  194.2 383.4 %all_to_all.33 = bf16[64,32,4096]{2,1,0:T(8,128)(2,1)} all-to-all(bf16[64,32,4096]{2,1,0:T(8,128)(2,1)S(1)} %stack.2), channel_id=1, replica_groups=mesh['sp_0'=8,'sp_1'=4,'sp_2'=2,'tp'=4] {'sp_0','sp_1','sp_2'}, dimensions={0} | all-to-all | bytes 33554432 | tf_op jit(solution)/shard_map/all_to_all | solution.py:28
  577.5 16.6 %fusion.24 = bf16[512,2048]{1,0:T(8,128)(2,1)} fusion(bf16[2048,4096]{1,0:T(8,128)(2,1)} %bitcast.687, bf16[512,2048]{0,1:T(8,128)(2,1)} %bitcast.142), kind=kOutput, calls=%fused_computation.56 | convolution fusion | flops 8594128896 | bytes 20971520 | tf_op jit(solution)/shard_map/dot_general | solution.py:273
  594.1 1.8 copy.230
  595.9 26.7 %all_to_all.34 = bf16[4,512,512]{2,1,0:T(8,128)(2,1)S(1)} all-to-all(bf16[4,512,512]{2,1,0:T(8,128)(2,1)S(1)} %bitcast.690), channel_id=1, replica_groups=mesh['sp_0'=8,'sp_1'=4,'sp_2'=2,'tp'=4] {'tp'}, dimensions={0} | all-to-all | bytes 4194304 | tf_op jit(solution)/shard_map/all_to_all | solution.py:101
  (236 shorter events, 41.2 us)
Async XLA Ops:
  6.5 129.1 %copy-start = (bf16[256,2048]{1,0:T(8,128)(2,1)S(1)}, bf16[256,2048]{1,0:T(8,128)(2,1)}, u32[]{:S(2)}) copy-start(bf16[256,2048]{1,0:T(8,128)(2,1)} %param.26) | copy-start | bytes 3145732
  6.5 3.5 copy-start.5
  6.5 4.1 copy-start.6
  6.5 4.1 copy-start.7
  6.5 111.8 %all-gather.11.cloned.1.call-start = ((), (), s32[]{:S(2)}) async-start(), calls=%async_computation.6 | async-start | bytes 1216512 | tf_op jit(solution)/shard_map/all_gather | solution.py:53
  10.7 26.1 %copy-start.16 = (u32[256]{0:T(256)S(1)}, u32[256]{0:T(256)}, u32[]{:S(2)}) copy-start(u32[256]{0:T(256)} %constant.114) | copy-start | bytes 3076
  10.7 36.1 %copy-start.15 = (u32[256]{0:T(256)S(1)}, u32[256]{0:T(256)}, u32[]{:S(2)}) copy-start(u32[256]{0:T(256)} %constant.119) | copy-start | bytes 3076
  36.7 44.3 %copy-start.14 = (u32[256]{0:T(256)S(1)}, u32[256]{0:T(256)}, u32[]{:S(2)}) copy-start(u32[256]{0:T(256)} %constant.124) | copy-start | bytes 3076
  79.2 36.5 %copy-start.8 = (f32[2]{0:T(128)}, f32[2]{0:T(128)S(1)}, u32[]{:S(2)}) copy-start(f32[2]{0:T(128)S(1)} %get-tuple-element.374) | copy-start | bytes 28
  119.4 2.6 copy-start.11
  120.7 4.2 copy-start.9
  122.0 2.8 copy-start.12
  124.8 6.6 %copy-start.13 = (bf16[256]{0:T(256)(128)(2,1)S(1)}, bf16[256]{0:T(256)(128)(2,1)}, u32[]{:S(2)}) copy-start(bf16[256]{0:T(256)(128)(2,1)} %param.25) | copy-start | bytes 1540
  127.5 8.1 %all-to-all-start = ((f32[4,1,512]{2,1,0:T(1,128)}), f32[4,1,512]{2,1,0:T(1,128)S(1)}, u32[]{:S(2)}, u32[]{:S(2)}) async-start(f32[4,1,512]{2,1,0:T(1,128)} %broadcast_in_dim.110), calls=%async_computation | async-start | bytes 16384 | tf_op jit(solution)/shard_map/all_to_all | solution.py:16
  159.2 1.0 copy-start.2
  160.3 4.2 copy-start.10
  161.2 7.4 %all-to-all-start.2 = ((f32[4,1,512]{2,1,0:T(1,128)}), f32[4,1,512]{2,1,0:T(1,128)S(1)}, u32[]{:S(2)}, u32[]{:S(2)}) async-start(f32[4,1,512]{2,1,0:T(1,128)} %broadcast_in_dim.111), calls=%async_computation.2 | async-start | bytes 16384 | tf_op jit(solution)/shard_map/all_to_all | solution.py:16
  170.6 4.6 copy-start.3
  170.6 4.6 copy-start.4
  170.6 21.5 %all-to-all-start.3 = ((bf16[4,512,512]{1,2,0:T(8,128)(2,1)}), bf16[4,512,512]{1,2,0:T(8,128)(2,1)}, u32[]{:S(2)}, u32[]{:S(2)}) async-start(bf16[4,512,512]{1,2,0:T(8,128)(2,1)} %broadcast_in_dim.112), calls=%async_computation.3 | async-start | bytes 4194304 | tf_op jit(solution)/shard_map/all_to_all | solution.py:16
  595.9 27.9 %copy-start.1 = (bf16[256,2048]{1,0:T(8,128)(2,1)S(1)}, bf16[256,2048]{1,0:T(8,128)(2,1)}, u32[]{:S(2)}) copy-start(bf16[256,2048]{1,0:T(8,128)(2,1)} %param.26) | copy-start | bytes 3145732
Sparse Core Ops, SparseCore 0:
  80.5 37.8 all-gather.10
